TPU v7x, 32 devices: a whole 2x2x4 slice. The times are simulated.
32 devices in a mesh: sp: 8 (over z, x), tp: 4 (over y, core).
Axes of the slice: x: 2, y: 2, z: 4, core: 2. Of those that a mesh axis runs over, the one named last changes fastest.
Arguments:
- queries: bfloat16 [5120, 2048], P('sp', 'tp'), may hold values from -164 to 164
- keys: bfloat16 [5120, 512], P('sp', 'tp'), may hold values from -6 to 6
- values: bfloat16 [5120, 512], P('sp', 'tp'), may hold values from -6 to 6
- sink: float32 [32], P('tp'), may hold values from 4 to 8
- stream: bfloat16 [5120, 2048], P(('sp', 'tp')), may hold values from -6 to 6
- out_weight: bfloat16 [2048, 2048], P('tp'), may hold values from -0.5390625 to 0.5390625
- norm_gain: float32 [2048], replicated, may hold values from 0.1 to 1.9
- gate_weight: bfloat16 [2048, 5632], P('sp', 'tp'), may hold values from -0.125 to 0.125
- up_weight: bfloat16 [2048, 5632], P('sp', 'tp'), may hold values from -0.125 to 0.125
- down_weight: bfloat16 [5632, 2048], P('tp', 'sp'), may hold values from -0.23925781 to 0.23925781
Outputs:
- result: bfloat16 [5120, 2048], P(('sp', 'tp'))
All inputs are finite; a program needn't handle non-finite values.
Results may differ from a plain program's by a relative error of at most 0.019.
Values may be sent and summed in bfloat16 or wider, within the bound.
A program may use at most 128 MiB of HBM per device.

v0:
```python
import functools

import jax
import jax.numpy as jnp
from jax import lax
from jax.experimental import pallas as pl
from jax.experimental.pallas import tpu as pltpu
from jax.sharding import PartitionSpec as P

HEAD = 64
WINDOW = 128
LANES = 128
BF = jnp.bfloat16
F32 = jnp.float32
MESH = pl.DeviceIdType.MESH


def padded_2(cells, sides, width):
    for axis, dim in sides:
        count = lax.axis_size(axis)
        ends = count - 1
        head = lax.slice_in_dim(cells, 0, width, axis=dim)
        tail = lax.slice_in_dim(cells, cells.shape[dim] - width, cells.shape[dim], axis=dim)
        cells = jnp.concatenate(
            [
                lax.ppermute(tail, axis, [(i, (i + 1) % count) for i in range(ends)]),
                cells,
                lax.ppermute(head, axis, [((i + 1) % count, i) for i in range(ends)]),
            ],
            axis=dim,
        )
    return cells


def rotary(block, start):
    length = block.shape[0]
    middle = HEAD // 2
    inverse = 1.0 / 10000.0 ** (jnp.arange(0, HEAD, 2, dtype=jnp.float32) / HEAD)
    places = (start + jnp.arange(length, dtype=jnp.int32)).astype(jnp.float32)
    angles = places[:, None, None] * inverse[None, None, :]
    cosine_table = jnp.cos(angles)
    sine_table = jnp.sin(angles)
    pieces = block.astype(jnp.float32).reshape(length, -1, HEAD)
    leading = pieces[..., :middle]
    trailing = pieces[..., middle:]
    turned = jnp.concatenate(
        [
            leading * cosine_table - trailing * sine_table,
            trailing * cosine_table + leading * sine_table,
        ],
        -1,
    )
    return turned.reshape(length, -1).astype(jnp.bfloat16)


def window_attend(queries, keys, values, sink):
    rows_here = queries.shape[0]
    start = lax.axis_index("sp") * rows_here
    length = lax.axis_size("sp") * rows_here
    blocks = rows_here // WINDOW
    kv_width = keys.shape[1]
    kv_count = kv_width // HEAD
    head_count = queries.shape[1] // HEAD
    group = head_count // kv_count
    turned_q = rotary(queries, start)
    turned_k = rotary(keys, start)
    paired = jnp.concatenate([turned_k, values], 1)
    padded = padded_2(paired, (("sp", 0),), WINDOW)
    framed = padded.reshape(blocks + 2, WINDOW, 2 * kv_width)
    banded = jnp.concatenate([framed[:-2], framed[1:-1], framed[2:]], axis=1)
    key_band = banded[..., :kv_width].reshape(blocks, 3 * WINDOW, kv_count, HEAD)
    value_band = banded[..., kv_width:].reshape(blocks, 3 * WINDOW, kv_count, HEAD)
    query_blocks = turned_q.reshape(blocks, WINDOW, kv_count, group, HEAD)
    scores = jnp.einsum(
        "nqkgd,nskd->nkgqs", query_blocks, key_band, preferred_element_type=jnp.float32
    ) * HEAD ** (-0.5)
    query_place = (
        start + jnp.arange(blocks)[:, None, None] * WINDOW + jnp.arange(WINDOW)[None, :, None]
    )
    key_place = (
        start
        + jnp.arange(blocks)[:, None, None] * WINDOW
        - WINDOW
        + jnp.arange(3 * WINDOW)[None, None, :]
    )
    valid = (jnp.abs(key_place - query_place) <= WINDOW) & (key_place >= 0) & (key_place < length)
    scores = jnp.where(valid[:, None, None], scores, -jnp.inf)
    sink_grid = sink.reshape(kv_count, group)[None, :, :, None]
    top = jnp.maximum(jnp.max(scores, -1), sink_grid)
    raised = jnp.exp(scores - top[..., None])
    denom = jnp.sum(raised, -1) + jnp.exp(sink_grid - top)
    weights = (raised / denom[..., None]).astype(jnp.bfloat16)
    output = jnp.einsum(
        "nkgqs,nskd->nqkgd", weights, value_band, preferred_element_type=jnp.float32
    )
    return output.astype(jnp.bfloat16).reshape(rows_here, head_count * HEAD)


def collect_weights(gate_weight, up_weight, down_weight):
    return (
        lax.all_gather(gate_weight, "sp", axis=0, tiled=True),
        lax.all_gather(up_weight, "sp", axis=0, tiled=True),
        lax.all_gather(down_weight, "sp", axis=1, tiled=True),
    )


def local(
    queries, keys, values, sink, stream, out_weight, norm_gain, gate_weight, up_weight, down_weight
):
    attended = window_attend(queries, keys, values, sink)
    gathered = collect_weights(gate_weight, up_weight, down_weight)
    gate_whole, up_whole, down_whole = gathered
    rows = attended
    projected = lax.psum_scatter(
        jnp.dot(rows, out_weight, preferred_element_type=jnp.float32),
        "tp",
        scatter_dimension=0,
        tiled=True,
    )
    mixed = (stream.astype(jnp.float32) + projected).astype(jnp.bfloat16)
    mixed_wide = mixed.astype(jnp.float32)
    scale = lax.rsqrt(jnp.mean(mixed_wide * mixed_wide, -1, keepdims=True) + 1e-06)
    normed = (mixed_wide * scale * norm_gain).astype(jnp.bfloat16)
    piece = lax.all_gather(normed, "tp", axis=0, tiled=True)
    gate = jnp.dot(piece, gate_whole, preferred_element_type=jnp.float32)
    upward = jnp.dot(piece, up_whole, preferred_element_type=jnp.float32)
    hidden = (jax.nn.silu(gate) * upward).astype(jnp.bfloat16)
    rows = hidden
    lowered = lax.psum_scatter(
        jnp.dot(rows, down_whole, preferred_element_type=jnp.float32).astype(jnp.bfloat16),
        "tp",
        scatter_dimension=0,
        tiled=True,
    ).astype(jnp.float32)
    return (mixed_wide + 0.5 * lowered).astype(jnp.bfloat16)


def turn_tables(length, start):
    lane = jnp.arange(LANES)
    pair = (lane % (HEAD // 2)).astype(F32) * 2.0
    inverse = 1.0 / 10000.0 ** (pair / HEAD)
    places = (start + jnp.arange(length, dtype=jnp.int32)).astype(F32)
    angles = places[:, None] * inverse[None, :]
    side = jnp.where(lane % HEAD < HEAD // 2, -1.0, 1.0).astype(F32)
    return jnp.cos(angles), jnp.sin(angles) * side[None, :]


def turned(block, cosine, sine):
    cells = block.astype(F32)
    lane = lax.broadcasted_iota(jnp.int32, cells.shape, 1)
    ahead = pltpu.roll(cells, LANES - HEAD // 2, 1)
    behind = pltpu.roll(cells, HEAD // 2, 1)
    other = jnp.where(lane % HEAD < HEAD // 2, ahead, behind)
    return (cells * cosine + other * sine).astype(BF)


def layer_kernel(
    dims, q_ref, kv_ref, cos_ref, sin_ref, sink_ref, stream_ref, w_ref, gain_ref, gu_own, gu_send, d_own, d_send,
    out_ref,
    kv, att, near, far, p_send, p_recv, kept, y_send, y_recv, mixed, na, nb, gu, dn,
    hid, c_send, c_recv, acc, s1a, r1a, s1b, r1b, s2a, r2a, s2b, r2b,
    gu_rs, d_rs, z_ss, x_ss, h_ss, h_rs, p_ss, p_rs, n_ss, n_rs, e_ss, e_rs,
):
    length, tokens, rows, per, tail, total = dims
    s = lax.axis_index("sp")
    z, x = s // 2, s % 2
    t = lax.axis_index("tp")
    y, c = t // 2, t % 2
    across = s + 1 - 2 * x
    at_x = {"sp": across}
    at_y = {"tp": t + 2 - 4 * y}
    at_c = {"tp": t + 1 - 2 * c}
    has_up, has_down = z < length - 1, z > 0
    last = 2 * length - 1

    def send(src, dst, ssem, rsem, to):
        return pltpu.make_async_remote_copy(
            src_ref=src, dst_ref=dst, send_sem=ssem, recv_sem=rsem,
            device_id=to, device_id_type=MESH,
        )

    barrier = pltpu.get_barrier_semaphore()

    def greet(to):
        pl.semaphore_signal(barrier, inc=1, device_id=to, device_id_type=MESH)

    greet(at_x)
    greet(at_y)
    greet(at_c)
    pl.when(has_up)(lambda: greet({"sp": s + 2}))
    pl.when(has_down)(lambda: greet({"sp": s - 2}))
    hop_up = (x == 1) & has_up
    hop_down = (x == 0) & has_down
    pl.when(hop_up)(lambda: greet({"sp": s + 1}))
    pl.when(hop_down)(lambda: greet({"sp": s - 1}))
    count = 3 + has_up.astype(jnp.int32) + has_down.astype(jnp.int32)
    count = count + hop_up.astype(jnp.int32) + hop_down.astype(jnp.int32)
    pl.semaphore_wait(barrier, count)

    after = send(kv_ref.at[pl.ds(tokens - WINDOW, WINDOW)], kv.at[pl.ds(0, WINDOW)], h_ss.at[0], h_rs.at[0], {"sp": s + 1})
    before = send(kv_ref.at[pl.ds(0, WINDOW)], kv.at[pl.ds(tokens + WINDOW, WINDOW)], h_ss.at[1], h_rs.at[1], {"sp": s - 1})
    pl.when(s < last)(after.start)
    pl.when(s > 0)(before.start)

    x_gu = send(gu_send, gu.at[s], x_ss.at[0], gu_rs.at[s], at_x)
    x_d = send(d_send, dn.at[s], x_ss.at[1], d_rs.at[s], at_x)
    x_gu.start()

    def line(kind, src, slot, index, side, way):
        buf, sems = ((gu, gu_rs), (dn, d_rs))[kind]
        to = {"sp": s + 2} if way == 0 else {"sp": s - 2}
        return send(src, buf.at[slot], z_ss.at[kind, way, index, side], sems.at[slot], to)

    def at_index(index):
        if index == 0:
            return z
        tables = ((0, 1, 2, 3), (1, 0, 2, 3), (2, 3, 1, 0), (3, 2, 1, 0))
        place = jnp.int32(tables[length - 1][index])
        for k in range(length - 1):
            place = jnp.where(z == k, tables[k][index], place)
        return place

    def landed(kind, slot):
        buf, sems = ((gu, gu_rs), (dn, d_rs))[kind]
        send(buf.at[slot], buf.at[slot], x_ss.at[0], sems.at[slot], at_x).wait_recv()

    def ways(index):
        if index == 0:
            return (has_up, has_down)
        place = at_index(index)
        return ((place < z) & has_up, (place > z) & has_down)

    def slot_of(index, side):
        return 2 * at_index(index) + (x if side == 0 else 1 - x)

    def push(kind, index, side):
        slot = slot_of(index, side)
        own = index == 0 and side == 0
        buf = (gu, dn)[kind]
        if not own:
            landed(kind, slot)
        src = (gu_own, d_own)[kind] if own else buf.at[slot]
        for way, cond in enumerate(ways(index)):
            pl.when(cond)(line(kind, src, slot, index, side, way).start)

    middle = has_up & has_down

    def relay(kind, index, side):
        pl.when(middle)(lambda: push(kind, index, side))

    def settle(kind, index, side):
        pl.when(jnp.logical_not(middle))(lambda: landed(kind, slot_of(index, side)))

    push(0, 0, 0)
    push(1, 0, 0)
    x_d.start()
    kv[pl.ds(WINDOW, tokens), :] = kv_ref[...]
    gu[s] = gu_own[...]
    dn[s] = d_own[...]

    @pl.when(s == 0)
    def _():
        kv[pl.ds(0, WINDOW), :] = jnp.zeros((WINDOW, kv.shape[1]), BF)

    @pl.when(s == last)
    def _():
        kv[pl.ds(tokens + WINDOW, WINDOW), :] = jnp.zeros((WINDOW, kv.shape[1]), BF)

    pl.when(s > 0)(after.wait_recv)
    pl.when(s < last)(before.wait_recv)

    kv_width = kv.shape[1] // 2
    heads = q_ref.shape[1] // HEAD

    def turn_keys(n, carry):
        at = pl.ds(pl.multiple_of(n * WINDOW, WINDOW), WINDOW)
        for p in range(kv_width // LANES):
            cols = slice(p * LANES, (p + 1) * LANES)
            kv[at, cols] = turned(kv[at, cols], cos_ref[at, :], sin_ref[at, :])
        return carry

    lax.fori_loop(0, tokens // WINDOW + 2, turn_keys, 0)
    group = heads // (kv_width // HEAD)

    def attend(n, carry):
        base = pl.multiple_of(n * WINDOW, WINDOW)
        shape = (WINDOW, 3 * WINDOW)
        q_at = lax.broadcasted_iota(jnp.int32, shape, 0)
        k_at = lax.broadcasted_iota(jnp.int32, shape, 1) - WINDOW
        place = k_at + (s * tokens + base)
        valid = (jnp.abs(k_at - q_at) <= WINDOW) & (place >= 0) & (place < total)
        outs = []
        for h in range(heads):
            g = h // group
            if h % 2 == 0:
                here = pl.ds(pl.multiple_of(base + WINDOW, WINDOW), WINDOW)
                two = q_ref[pl.ds(base, WINDOW), h * HEAD : (h + 2) * HEAD]
                two = turned(two, cos_ref[here, :], sin_ref[here, :])
            q = two[:, HEAD * (h % 2) : HEAD * (h % 2 + 1)]
            k = kv[pl.ds(base, 3 * WINDOW), g * HEAD : (g + 1) * HEAD]
            v = kv[pl.ds(base, 3 * WINDOW), kv_width + g * HEAD : kv_width + (g + 1) * HEAD]
            sc = lax.dot_general(q, k, (((1,), (1,)), ((), ())), preferred_element_type=F32)
            sc = jnp.where(valid, sc * HEAD ** (-0.5), -jnp.inf)
            sink = sink_ref[h]
            top = jnp.maximum(jnp.max(sc, -1, keepdims=True), sink)
            raised = jnp.exp(sc - top)
            denom = jnp.sum(raised, -1, keepdims=True) + jnp.exp(sink - top)
            weights = (raised / denom).astype(BF)
            outs.append(jnp.dot(weights, v, preferred_element_type=F32).astype(BF))
            if h % 2:
                att[pl.ds(base, WINDOW), (h - 1) * HEAD : (h + 1) * HEAD] = jnp.concatenate(outs[-2:], 1)
        return carry

    blocks = tokens // WINDOW
    def between(n, carry):
        attend(n, carry)

        @pl.when(n == blocks - 3)
        def _():
            push(0, 0, 1)

        @pl.when(n == blocks - 2)
        def _():
            relay(0, 1, 0)
            relay(0, 2, 0)

        return carry

    lax.fori_loop(0, blocks, between, 0)
    push(1, 0, 1)

    for dy in range(2):
        yy = y if dy == 0 else 1 - y
        mine = pl.multiple_of((2 * yy + c) * rows, 32)
        theirs = pl.multiple_of((2 * yy + 1 - c) * rows, 32)
        near[pl.ds(dy * rows, rows), :] = att[pl.ds(mine, rows), :]
        far[pl.ds(dy * rows, rows), :] = att[pl.ds(theirs, rows), :]
    model = out_ref.shape[1]
    step = 4 * LANES

    def project_far(n, carry):
        cols = pl.ds(pl.multiple_of(n * step, step), step)
        p_send[:, cols] = jnp.dot(far[...], w_ref[:, cols], preferred_element_type=F32).astype(BF)
        return carry

    def project_near(n, carry):
        cols = pl.ds(pl.multiple_of(n * step, step), step)
        kept[:, cols] = jnp.dot(near[...], w_ref[:, cols], preferred_element_type=F32)
        return carry

    lax.fori_loop(0, model // step, project_far, 0)
    by_core = send(p_send, p_recv, p_ss.at[0], p_rs.at[0], at_c)
    by_core.start()
    lax.fori_loop(0, model // step, project_near, 0)
    by_core.wait_recv()
    y_send[...] = (kept[rows:, :] + p_recv[rows:, :].astype(F32)).astype(BF)
    by_y = send(y_send, y_recv, p_ss.at[1], p_rs.at[1], at_y)
    by_y.start()
    relay(0, 1, 1)
    relay(0, 2, 1)
    by_y.wait_recv()
    mix = stream_ref[...].astype(F32) + (kept[:rows, :] + p_recv[:rows, :].astype(F32) + y_recv[...].astype(F32))
    mix = mix.astype(BF)
    mixed[...] = mix
    wide = mix.astype(F32)
    scale = lax.rsqrt(jnp.mean(wide * wide, -1, keepdims=True) + 1e-06)
    normed = (wide * scale * gain_ref[...]).astype(BF)
    cut = model // 2
    na[0, 0] = normed[:, :cut]
    nb[0, 0] = normed[:, cut:]

    a_x = send(na.at[0, 0], na.at[0, 1], n_ss.at[0], n_rs.at[0], at_x)
    b_y = send(nb.at[0, 0], nb.at[0, 2], n_ss.at[1], n_rs.at[1], at_y)
    a_y0 = send(na.at[0, 0], na.at[0, 2], n_ss.at[2], n_rs.at[2], at_y)
    a_y1 = send(na.at[0, 1], na.at[0, 3], n_ss.at[3], n_rs.at[3], at_y)
    b_x0 = send(nb.at[0, 0], nb.at[0, 1], n_ss.at[4], n_rs.at[4], at_x)
    b_x1 = send(nb.at[0, 2], nb.at[0, 3], n_ss.at[5], n_rs.at[5], at_x)
    a_x.start()
    b_y.start()
    a_y0.start()
    b_x0.start()
    relay(0, 3, 0)
    a_x.wait_recv()
    a_y1.start()
    b_y.wait_recv()
    b_x1.start()
    a_y0.wait_recv()
    a_y1.wait_recv()
    b_x0.wait_recv()
    b_x1.wait_recv()
    a_c = send(na.at[0], na.at[1], n_ss.at[6], n_rs.at[6], at_c)
    b_c = send(nb.at[0], nb.at[1], n_ss.at[7], n_rs.at[7], at_c)
    a_c.start()
    b_c.start()
    relay(0, 3, 1)
    for index in (1, 2):
        for side in range(2):
            relay(1, index, side)
    for index in range(1, length):
        for side in range(2):
            settle(0, index, side)

    def units(q, cols, size):
        half = size // 2
        depth = gu.shape[1]
        lhs = na[q].reshape(4 * rows, cut)
        rhs = nb[q].reshape(4 * rows, cut)
        one = gu[pl.ds(0, length), :, cols].reshape(length * depth, size)
        two = gu[pl.ds(length, length), :, cols].reshape(length * depth, size)
        both = jnp.dot(lhs, one, preferred_element_type=F32) + jnp.dot(rhs, two, preferred_element_type=F32)
        gate = both[:, :half]
        return (gate / (1.0 + jnp.exp(-gate)) * both[:, half:]).astype(BF)

    def hidden_of(q):
        def body(n, carry):
            cols = pl.ds(pl.multiple_of(n * 2 * LANES, 2 * LANES), 2 * LANES)
            hid[q, :, pl.ds(pl.multiple_of(n * LANES, LANES), LANES)] = units(q, cols, 2 * LANES)
            return carry

        lax.fori_loop(0, per, body, 0)
        hid[q, :, per * LANES :] = units(q, pl.ds(per * 2 * LANES, 2 * tail), 2 * tail)

    hidden_of(0)
    relay(1, 3, 0)
    a_c.wait_recv()
    b_c.wait_recv()
    hidden_of(1)
    relay(1, 3, 1)

    part = d_own.shape[1]

    def exchange(k, which):
        src, dst, to = (
            (c_send.at[k], c_recv.at[k], at_c),
            (s1a.at[k], r1a.at[k], at_x),
            (s1b.at[k], r1b.at[k], at_y),
            (s2a.at[k], r2a.at[k], at_y),
            (s2b.at[k], r2b.at[k], at_x),
        )[which]
        return send(src, dst, e_ss.at[which, k], e_rs.at[which, k], to)

    def second(k):
        exchange(k, 1).wait_recv()
        exchange(k, 2).wait_recv()
        a = [acc[k, 0, 2 * dy] + r1a[k, dy].astype(F32) for dy in range(2)]
        b = [acc[k, 1, dx] + r1b[k, dx].astype(F32) for dx in range(2)]
        s2a[k] = a[1].astype(BF)
        s2b[k] = b[1].astype(BF)
        exchange(k, 3).start()
        exchange(k, 4).start()
        acc[k, 0, 0] = a[0]
        acc[k, 1, 0] = b[0]

    for k in range(length):
        if k:
            settle(1, k, 0)
            settle(1, k, 1)
        low = 2 * at_index(k)
        for side in range(2):
            weight = dn[low + side]
            c_send[k, side] = jnp.dot(hid[1], weight, preferred_element_type=F32).astype(BF)
        exchange(k, 0).start()
        for side in range(2):
            weight = dn[low + side]
            acc[k, side] = jnp.dot(hid[0], weight, preferred_element_type=F32).reshape(4, rows, part)
        if k:
            second(k - 1)
        exchange(k, 0).wait_recv()
        acc[k] = acc[k] + c_recv[k].reshape(2, 4, rows, part).astype(F32)
        for dy in range(2):
            s1a[k, dy] = acc[k, 0, 2 * dy + 1].astype(BF)
        for dx in range(2):
            s1b[k, dx] = acc[k, 1, 2 + dx].astype(BF)
        exchange(k, 1).start()
        exchange(k, 2).start()
    second(length - 1)
    for k in range(length):
        exchange(k, 3).wait_recv()
        exchange(k, 4).wait_recv()
        for side, got in ((0, r2a), (1, r2b)):
            cols = pl.ds(pl.multiple_of((2 * at_index(k) + side) * part, part), part)
            lowered = acc[k, side, 0] + got[k].astype(F32)
            out_ref[:, cols] = (mixed[:, cols].astype(F32) + 0.5 * lowered).astype(BF)

    pl.when(s < last)(after.wait_send)
    pl.when(s > 0)(before.wait_send)
    for copy in (x_gu, x_d, by_core, by_y, a_x, b_y, a_y0, a_y1, b_x0, b_x1, a_c, b_c):
        copy.wait_send()
    for k in range(length):
        for which in range(5):
            exchange(k, which).wait_send()
    for kind in range(2):
        for index in range(length):
            for side in range(2):
                slot = slot_of(index, side)
                own = index == 0 and side == 0
                src = (gu_own, d_own)[kind] if own else (gu, dn)[kind].at[slot]
                for way, cond in enumerate(ways(index)):
                    pl.when(cond)(line(kind, src, slot, index, side, way).wait_send)


def local_lines(
    queries, keys, values, sink, stream, out_weight, norm_gain, gate_weight, up_weight, down_weight
):
    length = lax.axis_size("sp") // 2
    s = lax.axis_index("sp")
    tokens = queries.shape[0]
    rows, model = stream.shape
    depth, wide = gate_weight.shape
    per = wide // LANES // 2
    tail = wide // 2 - per * LANES
    half = wide // 2
    edge = 2 * per * LANES

    def pieces(x):
        out = []
        for n in range(per):
            at = (x * per + n) * LANES
            out += [gate_weight[:, at : at + LANES], up_weight[:, at : at + LANES]]
        at = edge + x * tail
        out += [gate_weight[:, at : at + tail], up_weight[:, at : at + tail]]
        return jnp.concatenate(out, 1)

    def lowers(x):
        at = x * per * LANES
        end = edge + x * tail
        return jnp.concatenate([down_weight[at : at + per * LANES], down_weight[end : end + tail]], 0)

    first = s % 2 == 0
    gu_0, gu_1, d_0, d_1 = pieces(0), pieces(1), lowers(0), lowers(1)
    paired = jnp.concatenate([keys, values], 1)
    cosine, sine = turn_tables(tokens + 2 * WINDOW, s * tokens - WINDOW)
    part = down_weight.shape[1]
    vmem = pl.BlockSpec(memory_space=pltpu.VMEM)
    dma = pltpu.SemaphoreType.DMA
    dims = (length, tokens, rows, per, tail, tokens * 2 * length)
    return pl.pallas_call(
        functools.partial(layer_kernel, dims),
        out_shape=jax.ShapeDtypeStruct((rows, model), BF),
        in_specs=[vmem] * 4 + [pl.BlockSpec(memory_space=pltpu.SMEM)] + [vmem] * 7,
        out_specs=vmem,
        scratch_shapes=[
            pltpu.VMEM((tokens + 2 * WINDOW, paired.shape[1]), BF),
            pltpu.VMEM(queries.shape, BF),
            pltpu.VMEM((2 * rows, queries.shape[1]), BF),
            pltpu.VMEM((2 * rows, queries.shape[1]), BF),
            pltpu.VMEM((2 * rows, model), BF),
            pltpu.VMEM((2 * rows, model), BF),
            pltpu.VMEM((2 * rows, model), F32),
            pltpu.VMEM((rows, model), BF),
            pltpu.VMEM((rows, model), BF),
            pltpu.VMEM((rows, model), BF),
            pltpu.VMEM((2, 4, rows, model // 2), BF),
            pltpu.VMEM((2, 4, rows, model // 2), BF),
            pltpu.VMEM((2 * length, depth, 2 * half), BF),
            pltpu.VMEM((2 * length, half, part), BF),
            pltpu.VMEM((2, 4 * rows, half), BF),
            pltpu.VMEM((length, 2, 4 * rows, part), BF),
            pltpu.VMEM((length, 2, 4 * rows, part), BF),
            pltpu.VMEM((length, 2, 4, rows, part), F32),
        ]
        + [pltpu.VMEM((length, 2, rows, part), BF)] * 4
        + [pltpu.VMEM((length, rows, part), BF)] * 4
        + [
            dma((2 * length,)), dma((2 * length,)), dma((2, 2, length, 2)), dma((2,)),
            dma((2,)), dma((2,)), dma((2,)), dma((2,)), dma((8,)), dma((8,)),
            dma((5, length)), dma((5, length)),
        ],
        compiler_params=pltpu.CompilerParams(
            collective_id=0, has_side_effects=True, vmem_limit_bytes=63 * 1024 * 1024
        ),
    )(
        queries, paired, cosine, sine, sink, stream, out_weight, norm_gain[None],
        jnp.where(first, gu_0, gu_1), jnp.where(first, gu_1, gu_0),
        jnp.where(first, d_0, d_1), jnp.where(first, d_1, d_0),
    )


def solution(mesh):
    placed = (
        P("sp", "tp"),
        P("sp", "tp"),
        P("sp", "tp"),
        P("tp"),
        P(("sp", "tp"), None),
        P("tp", None),
        P(),
        P("sp", "tp"),
        P("sp", "tp"),
        P("tp", "sp"),
    )
    lines = mesh.shape["tp"] == 4 and mesh.shape["sp"] == 8
    return jax.shard_map(
        local_lines if lines else local, mesh=mesh, in_specs=placed, out_specs=P(("sp", "tp"), None), check_vma=False
    )
```

profile of v0, /device:TPU:0, one launch (start us, length us, event | category | flops | bytes accessed | tf_op | source)
XLA Modules:
  0.0 177.9 jit_solution(10282212328849217)
XLA Ops:
  0.0 0.0 copy-start
  0.0 0.8 fusion.6
  0.9 1.0 fusion.7
  1.9 1.8 pad_maximum_fusion.2.kv_ref
  3.7 0.0 copy-start.1
  3.7 1.2 fusion.5
  4.9 1.0 broadcast_select_fusion.2
  5.9 0.0 copy-done
  5.9 0.1 fusion.10
  6.0 0.0 copy-done.1
  6.0 0.1 fusion.9
  6.2 0.3 concatenate.17
  6.5 0.3 concatenate.16
  6.8 1.3 broadcast_select_fusion
  8.1 2.6 %fusion = (f32[896,128]{1,0:T(8,128)}, f32[896,128]{1,0:T(8,128)}) fusion(f32[128]{0:T(128)S(1)} %get-tuple-element.39, f32[128]{0:T(128)S(1)} %get-tuple-element.40, f32[896]{0:T(1024)S(1)} %add_convert_fusion), kind=kLoop, calls=%fused_computation.4 | loop fusion | flops 229376 | bytes 922112 | tf_op jit(solution)/shard_map/mul | solution.py:145
  10.7 165.2 %shard_map.100 = bf16[160,2048]{1,0:T(8,128)(2,1)} custom-call(bf16[640,512]{1,0:T(8,128)(2,1)} %q_ref.1, bf16[640,256]{1,0:T(8,128)(2,1)} %pad_maximum_fusion.2.kv_ref, f32[896,128]{1,0:T(8,128)} %get-tuple-element.38.cos_ref, f32[896,128]{1,0:T(8,128)} %get-tuple-element.37.sin_ref, f32[8]{0:T(128)} %sink_ref.1, bf16[160,2048]{1,0:T(8,128)(2,1)} %stream_ref.1, ...), custom_call_target="tpu_custom_call" | custom-call | tf_op jit(solution)/shard_map/pallas_call | solution.py:537
  175.9 2.0 %copy.12 = bf16[160,2048]{1,0:T(8,128)(2,1)} copy(bf16[160,2048]{1,0:T(8,128)(2,1)} %shard_map.100) | data formatting | bytes 1310720
  (2 shorter events, 0.0 us)
Async XLA Ops:
  0.0 5.9 %copy-start = (bf16[256,1408]{1,0:T(8,128)(2,1)S(1)}, bf16[256,1408]{1,0:T(8,128)(2,1)}, u32[]{:S(2)}) copy-start(bf16[256,1408]{1,0:T(8,128)(2,1)} %param.17) | copy-start | bytes 2162692
  3.7 2.3 %copy-start.1 = (bf16[256,1408]{1,0:T(8,128)(2,1)S(1)}, bf16[256,1408]{1,0:T(8,128)(2,1)}, u32[]{:S(2)}) copy-start(bf16[256,1408]{1,0:T(8,128)(2,1)} %param.18) | copy-start | bytes 2162692
where the time goes:
time: 178 us
  Pallas kernels  165 us (93%)
  other arithmetic  6.66 us (4%)
  local copies, waits for them, and re-layouts  5.93 us (3%)
    pallas_call x1, Pallas kernels, local_lines(): pl.pallas_call(functools.partial(layer_kernel, dims), out_shape=jax.Shape...  165 us

commit v1 on v0

v1 whole, which is shorter than its diff:
```python
import functools

import jax
import jax.numpy as jnp
import numpy as np
from jax import lax
from jax.experimental import pallas as pl
from jax.experimental.pallas import tpu as pltpu
from jax.sharding import PartitionSpec as P

HEAD = 64
WINDOW = 128
LANES = 128
BF = jnp.bfloat16
F32 = jnp.float32
MESH = pl.DeviceIdType.MESH


def padded_2(cells, sides, width):
    for axis, dim in sides:
        count = lax.axis_size(axis)
        ends = count - 1
        head = lax.slice_in_dim(cells, 0, width, axis=dim)
        tail = lax.slice_in_dim(cells, cells.shape[dim] - width, cells.shape[dim], axis=dim)
        cells = jnp.concatenate(
            [
                lax.ppermute(tail, axis, [(i, (i + 1) % count) for i in range(ends)]),
                cells,
                lax.ppermute(head, axis, [((i + 1) % count, i) for i in range(ends)]),
            ],
            axis=dim,
        )
    return cells


def rotary(block, start):
    length = block.shape[0]
    middle = HEAD // 2
    inverse = 1.0 / 10000.0 ** (jnp.arange(0, HEAD, 2, dtype=jnp.float32) / HEAD)
    places = (start + jnp.arange(length, dtype=jnp.int32)).astype(jnp.float32)
    angles = places[:, None, None] * inverse[None, None, :]
    cosine_table = jnp.cos(angles)
    sine_table = jnp.sin(angles)
    pieces = block.astype(jnp.float32).reshape(length, -1, HEAD)
    leading = pieces[..., :middle]
    trailing = pieces[..., middle:]
    turned = jnp.concatenate(
        [
            leading * cosine_table - trailing * sine_table,
            trailing * cosine_table + leading * sine_table,
        ],
        -1,
    )
    return turned.reshape(length, -1).astype(jnp.bfloat16)


def window_attend(queries, keys, values, sink):
    rows_here = queries.shape[0]
    start = lax.axis_index("sp") * rows_here
    length = lax.axis_size("sp") * rows_here
    blocks = rows_here // WINDOW
    kv_width = keys.shape[1]
    kv_count = kv_width // HEAD
    head_count = queries.shape[1] // HEAD
    group = head_count // kv_count
    turned_q = rotary(queries, start)
    turned_k = rotary(keys, start)
    paired = jnp.concatenate([turned_k, values], 1)
    padded = padded_2(paired, (("sp", 0),), WINDOW)
    framed = padded.reshape(blocks + 2, WINDOW, 2 * kv_width)
    banded = jnp.concatenate([framed[:-2], framed[1:-1], framed[2:]], axis=1)
    key_band = banded[..., :kv_width].reshape(blocks, 3 * WINDOW, kv_count, HEAD)
    value_band = banded[..., kv_width:].reshape(blocks, 3 * WINDOW, kv_count, HEAD)
    query_blocks = turned_q.reshape(blocks, WINDOW, kv_count, group, HEAD)
    scores = jnp.einsum(
        "nqkgd,nskd->nkgqs", query_blocks, key_band, preferred_element_type=jnp.float32
    ) * HEAD ** (-0.5)
    query_place = (
        start + jnp.arange(blocks)[:, None, None] * WINDOW + jnp.arange(WINDOW)[None, :, None]
    )
    key_place = (
        start
        + jnp.arange(blocks)[:, None, None] * WINDOW
        - WINDOW
        + jnp.arange(3 * WINDOW)[None, None, :]
    )
    valid = (jnp.abs(key_place - query_place) <= WINDOW) & (key_place >= 0) & (key_place < length)
    scores = jnp.where(valid[:, None, None], scores, -jnp.inf)
    sink_grid = sink.reshape(kv_count, group)[None, :, :, None]
    top = jnp.maximum(jnp.max(scores, -1), sink_grid)
    raised = jnp.exp(scores - top[..., None])
    denom = jnp.sum(raised, -1) + jnp.exp(sink_grid - top)
    weights = (raised / denom[..., None]).astype(jnp.bfloat16)
    output = jnp.einsum(
        "nkgqs,nskd->nqkgd", weights, value_band, preferred_element_type=jnp.float32
    )
    return output.astype(jnp.bfloat16).reshape(rows_here, head_count * HEAD)


def collect_weights(gate_weight, up_weight, down_weight):
    return (
        lax.all_gather(gate_weight, "sp", axis=0, tiled=True),
        lax.all_gather(up_weight, "sp", axis=0, tiled=True),
        lax.all_gather(down_weight, "sp", axis=1, tiled=True),
    )


def local(
    queries, keys, values, sink, stream, out_weight, norm_gain, gate_weight, up_weight, down_weight
):
    attended = window_attend(queries, keys, values, sink)
    gathered = collect_weights(gate_weight, up_weight, down_weight)
    gate_whole, up_whole, down_whole = gathered
    rows = attended
    projected = lax.psum_scatter(
        jnp.dot(rows, out_weight, preferred_element_type=jnp.float32),
        "tp",
        scatter_dimension=0,
        tiled=True,
    )
    mixed = (stream.astype(jnp.float32) + projected).astype(jnp.bfloat16)
    mixed_wide = mixed.astype(jnp.float32)
    scale = lax.rsqrt(jnp.mean(mixed_wide * mixed_wide, -1, keepdims=True) + 1e-06)
    normed = (mixed_wide * scale * norm_gain).astype(jnp.bfloat16)
    piece = lax.all_gather(normed, "tp", axis=0, tiled=True)
    gate = jnp.dot(piece, gate_whole, preferred_element_type=jnp.float32)
    upward = jnp.dot(piece, up_whole, preferred_element_type=jnp.float32)
    hidden = (jax.nn.silu(gate) * upward).astype(jnp.bfloat16)
    rows = hidden
    lowered = lax.psum_scatter(
        jnp.dot(rows, down_whole, preferred_element_type=jnp.float32).astype(jnp.bfloat16),
        "tp",
        scatter_dimension=0,
        tiled=True,
    ).astype(jnp.float32)
    return (mixed_wide + 0.5 * lowered).astype(jnp.bfloat16)


def turn_tables(blocks):
    lane = np.arange(LANES)
    inverse = 10000.0 ** (-2.0 * (lane % (HEAD // 2)) / HEAD)
    within = np.arange(WINDOW)[:, None] * inverse[None, :]
    begins = (np.arange(blocks) - 1)[:, None] * WINDOW * inverse[None, :]
    pair = lambda a: np.stack([np.cos(a), np.sin(a)]).astype(np.float32)
    return pair(within), pair(begins)


NAMES = "onfs"
GCH, DCH = 4, 4


def layer_kernel(
    dims, q_in, k_in, v_in, sink_ref, stream_in, w_in, gain_ref, gate_in, up_in, down_in, turn_ref, begin_ref,
    out_ref,
    qv, kv, kk, vv, att, wv, sv, tails, oth, doth, gu, dn, p_send, p_recv, kept, y_send, y_recv, mixed, nt,
    hid, c_send, c_recv, acc, s1, r1, s2, r2,
    loc, h_ss, h_rs, z_ss, x_ss, gu_rs, d_rs, p_ss, p_rs, n_ss, n_rs, e_ss, e_rs,
):
    length, tokens, rows, per, tail, total = dims
    s = lax.axis_index("sp")
    z, x = s // 2, s % 2
    t = lax.axis_index("tp")
    y, c = t // 2, t % 2
    part = z % 2
    pz = z + 1 - 2 * part
    half = length // 2
    flip = lambda q: q + half - 2 * half * (q // half)
    fz, fp = flip(z), flip(pz)
    dests = {"o": fz, "n": pz, "f": fp, "s": z}
    outer = (z == 0) | (z == length - 1)
    at_x = {"sp": s + 1 - 2 * x}
    at_n = {"sp": 2 * pz + x}
    at_y = {"tp": t + 2 - 4 * y}
    at_c = {"tp": t + 1 - 2 * c}
    last = 2 * length - 1
    model = out_ref.shape[1]
    blocks = tokens // WINDOW
    edge = per * 2 * LANES
    cut = per * LANES

    def send(src, dst, ssem, rsem, to):
        return pltpu.make_async_remote_copy(
            src_ref=src, dst_ref=dst, send_sem=ssem, recv_sem=rsem,
            device_id=to, device_id_type=MESH,
        )

    def fetch(src, dst, i):
        return pltpu.make_async_copy(src, dst, loc.at[i])

    def fetch_part(which, dst, i):
        for n in range(per):
            at = pl.multiple_of((which * per + n) * LANES, LANES)
            for side, src in ((0, gate_in), (1, up_in)):
                fetch(src.at[:, pl.ds(at, LANES)], dst.at[:, pl.ds((2 * n + side) * LANES, LANES)], i).start()

    def fetch_down(which, dst, i):
        fetch(down_in.at[pl.ds(pl.multiple_of(which * cut, LANES), cut)], dst.at[pl.ds(0, cut)], i).start()
        at = pl.multiple_of(edge + which * tail, tail)
        fetch(down_in.at[pl.ds(at, tail)], dst.at[pl.ds(cut, tail)], i).start()

    whole_k = fetch(k_in, kv.at[pl.ds(WINDOW, tokens), pl.ds(0, LANES)], 3)
    whole_v = fetch(v_in, kv.at[pl.ds(WINDOW, tokens), pl.ds(LANES, LANES)], 4)
    whole_q = fetch(q_in, qv, 5)
    whole_w = fetch(w_in, wv, 8)
    whole_s = fetch(stream_in, sv, 9)
    fetch_part(1 - part, oth, 0)
    fetch(gate_in.at[:, pl.ds(edge, LANES)], tails.at[0], 2).start()
    fetch(up_in.at[:, pl.ds(edge, LANES)], tails.at[1], 2).start()
    fetch_part(part, gu.at[s], 1)
    whole_k.start()
    whole_v.start()
    fetch_down(1 - part, doth, 7)
    whole_q.start()
    fetch_down(part, dn.at[s], 6)
    whole_w.start()
    whole_s.start()

    barrier = pltpu.get_barrier_semaphore()

    def greet(to):
        pl.semaphore_signal(barrier, inc=1, device_id=to, device_id_type=MESH)

    for to in (at_x, at_n, {"sp": 2 * fz + x}, {"sp": 2 * fp + x}, at_y, at_c):
        greet(to)
    hop_up = (x == 1) & (z < length - 1)
    hop_down = (x == 0) & (z > 0)
    pl.when(hop_up)(lambda: greet({"sp": s + 1}))
    pl.when(hop_down)(lambda: greet({"sp": s - 1}))
    pl.semaphore_wait(barrier, 6 + hop_up.astype(jnp.int32) + hop_down.astype(jnp.int32))

    halos = []
    for i, src in ((0, k_in), (1, v_in)):
        cols = pl.ds(i * LANES, LANES)
        after = send(src.at[pl.ds(tokens - WINDOW, WINDOW)], kv.at[pl.ds(0, WINDOW), cols], h_ss.at[0, i], h_rs.at[0, i], {"sp": s + 1})
        before = send(src.at[pl.ds(0, WINDOW)], kv.at[pl.ds(tokens + WINDOW, WINDOW), cols], h_ss.at[1, i], h_rs.at[1, i], {"sp": s - 1})
        pl.when(s < last)(after.start)
        pl.when(s > 0)(before.start)
        halos.append((after, before))

    chunks = (GCH, DCH)

    def piece(kind, ref, g):
        size = (gu, dn)[kind].shape[1] // chunks[kind]
        return ref.at[pl.ds(g * size, size)]

    def slot_of(name):
        return 2 * dests[name] + x

    def buffers(kind):
        return ((gu, gu_rs), (dn, d_rs))[kind]

    def by_z(kind, name, g):
        buf, got = buffers(kind)
        src = buf.at[s] if name == "o" else (oth, doth)[kind]
        sem = z_ss.at[kind, NAMES.index(name), g]
        return send(piece(kind, src, g), piece(kind, buf.at[s], g), sem, got.at[s, g], {"sp": slot_of(name)})

    def by_x(kind, name, g):
        buf, got = buffers(kind)
        here = piece(kind, buf.at[slot_of(name)], g)
        return send(here, here, x_ss.at[kind, NAMES.index(name), g], got.at[slot_of(name), g], at_x)

    def landed(kind, slot, g):
        buf, got = buffers(kind)
        here = piece(kind, buf.at[slot], g)
        send(here, here, x_ss.at[0, 0, 0], got.at[slot, g], at_x).wait_recv()

    def push(kind, name):
        for g in range(chunks[kind]):
            by_z(kind, name, g).start()

    def relay(kind, name, some=None):
        for g in range(chunks[kind]) if some is None else some:
            if name != "s":
                landed(kind, slot_of(name), g)
            by_x(kind, name, g).start()

    def crossed(kind, name):
        for g in range(chunks[kind]):
            landed(kind, 2 * dests[name] + 1 - x, g)

    fetch(oth.at[:, pl.ds(0, edge)], oth.at[:, pl.ds(0, edge)], 0).wait()
    fetch(tails, tails, 2).wait()
    low_tail = jnp.concatenate([tails[0, :, :tail], tails[1, :, :tail]], 1)
    high_tail = jnp.concatenate([tails[0, :, tail:], tails[1, :, tail:]], 1)
    oth[:, edge:] = jnp.where(part == 0, high_tail, low_tail)
    gu[s, :, edge:] = jnp.where(part == 0, low_tail, high_tail)
    push(0, "n")
    own = gu.at[s, :, pl.ds(0, edge)]
    fetch(own, own, 1).wait()
    relay(0, "s")
    fetch(doth, doth, 7).wait()
    push(1, "n")
    push(0, "o")
    pl.when(jnp.logical_not(outer))(lambda: push(0, "f"))
    fetch(dn.at[s], dn.at[s], 6).wait()

    lane = lax.broadcasted_iota(jnp.int32, (WINDOW, LANES), 1)
    low = lane < HEAD
    front = lane % HEAD < HEAD // 2

    def angles(m):
        row = s * blocks + m
        cos_b, sin_b = begin_ref[0, pl.ds(row, 1), :], begin_ref[1, pl.ds(row, 1), :]
        cosine = turn_ref[0] * cos_b - turn_ref[1] * sin_b
        sine = turn_ref[1] * cos_b + turn_ref[0] * sin_b
        return cosine, jnp.where(front, -sine, sine)

    def turned(block, cosine, sine):
        cells = block.astype(F32)
        other = jnp.where(front, pltpu.roll(cells, LANES - HEAD // 2, 1), pltpu.roll(cells, HEAD // 2, 1))
        return cells * cosine + other * sine

    def spread(m, carry):
        at = pl.ds(pl.multiple_of(m * WINDOW, WINDOW), WINDOW)
        cosine, sine = angles(m)
        for cells, dst in ((turned(kv[at, :LANES], cosine, sine), kk), (kv[at, LANES:].astype(F32), vv)):
            swapped = pltpu.roll(cells, HEAD, 1)
            dst[0, at, :] = jnp.where(low, cells, swapped).astype(BF)
            dst[1, at, :] = jnp.where(low, swapped, cells).astype(BF)
        return carry

    @pl.when(s == 0)
    def _():
        kv[pl.ds(0, WINDOW), :] = jnp.zeros((WINDOW, kv.shape[1]), BF)

    @pl.when(s == last)
    def _():
        kv[pl.ds(tokens + WINDOW, WINDOW), :] = jnp.zeros((WINDOW, kv.shape[1]), BF)

    whole_k.wait()
    whole_v.wait()
    lax.fori_loop(1, blocks + 1, spread, 0)
    for after, before in halos:
        pl.when(s > 0)(after.wait_recv)
        pl.when(s < last)(before.wait_recv)
    spread(0, 0)
    spread(blocks + 1, 0)
    whole_q.wait()

    heads = qv.shape[1] // HEAD
    kv_count = kk.shape[0]
    group = heads // kv_count
    firsts = (blocks + 1) // 2

    def attend(i, carry):
        n = jnp.where(i < firsts, blocks - firsts + i, blocks - 1 - i)
        n = jnp.where(y == 0, n, blocks - 1 - n)
        base = pl.multiple_of(n * WINDOW, WINDOW)
        shape = (WINDOW, 3 * WINDOW)
        q_at = lax.broadcasted_iota(jnp.int32, shape, 0)
        k_at = lax.broadcasted_iota(jnp.int32, shape, 1) - WINDOW
        place = k_at + (s * tokens + base)
        valid = (jnp.abs(k_at - q_at) <= WINDOW) & (place >= 0) & (place < total)
        cosine, sine = angles(n + 1)
        for g in range(kv_count):
            qs = []
            for j in range(group // 2):
                at = (g * group // 2 + j) * LANES
                two = turned(qv[pl.ds(base, WINDOW), at : at + LANES], cosine, sine).astype(BF) * BF(HEAD ** -0.5)
                qs += [jnp.where(low, two, BF(0)), jnp.where(low, BF(0), two)]
            k = kk[g, pl.ds(base, 3 * WINDOW), :]
            v = vv[g, pl.ds(base, 3 * WINDOW), :]
            scores = lax.dot_general(jnp.concatenate(qs, 0), k, (((1,), (1,)), ((), ())), preferred_element_type=F32)
            parts, shares = [], []
            for j in range(group):
                sc = jnp.where(valid, scores[j * WINDOW : (j + 1) * WINDOW], -jnp.inf)
                sink = sink_ref[g * group + j]
                top = jnp.maximum(jnp.max(sc, -1, keepdims=True), sink)
                raised = jnp.exp(sc - top)
                denom = jnp.sum(raised, -1, keepdims=True) + jnp.exp(sink - top)
                parts.append(raised.astype(BF))
                shares.append(1.0 / denom)
            outs = jnp.dot(jnp.concatenate(parts, 0), v, preferred_element_type=F32)
            outs = [outs[j * WINDOW : (j + 1) * WINDOW] * shares[j] for j in range(group)]
            for j in range(group // 2):
                at = (g * group // 2 + j) * LANES
                att[pl.ds(base, WINDOW), at : at + LANES] = jnp.where(low, outs[2 * j], outs[2 * j + 1]).astype(BF)
        return carry

    step = 4 * LANES
    wide = model // 2

    def project(which):
        begin = pl.multiple_of((y if which else 1 - y) * 2 * rows, 32)
        for m in range(2):
            def body(n, carry):
                cols = pl.ds(pl.multiple_of(m * wide + n * step, step), step)
                both = jnp.dot(att[pl.ds(begin, 2 * rows), :], wv[:, cols], preferred_element_type=F32)
                kept[which, :, :, cols] = both.reshape(2, rows, step)
                p_send[which, :, cols] = kept[which, 1 - c, :, cols].astype(BF)
                return carry

            lax.fori_loop(0, wide // step, body, 0)
            by_core(which, m).start()

    def by_core(which, m):
        cols = pl.ds(m * wide, wide)
        return send(p_send.at[which, :, cols], p_recv.at[which, :, cols], p_ss.at[which, m], p_rs.at[which, m], at_c)

    def by_y(m):
        cols = pl.ds(m * wide, wide)
        return send(y_send.at[:, cols], y_recv.at[:, cols], p_ss.at[2, m], p_rs.at[2, m], at_y)

    lax.fori_loop(0, firsts, attend, 0)
    whole_w.wait()
    project(0)
    lax.fori_loop(firsts, firsts + 1, attend, 0)
    for m in range(2):
        by_core(0, m).wait_recv()
        cols = slice(m * wide, (m + 1) * wide)
        y_send[:, cols] = (kept[0, c, :, cols] + p_recv[0, :, cols].astype(F32)).astype(BF)
        by_y(m).start()
    lax.fori_loop(firsts + 1, blocks, attend, 0)
    project(1)
    whole_s.wait()
    relay(0, "n")
    relay(1, "s")
    for m in range(2):
        by_core(1, m).wait_recv()
        by_y(m).wait_recv()
        cols = slice(m * wide, (m + 1) * wide)
        mix = kept[1, c, :, cols] + p_recv[1, :, cols].astype(F32) + y_recv[:, cols].astype(F32)
        mixed[:, cols] = (sv[:, cols].astype(F32) + mix).astype(BF)
    whole = mixed[...].astype(F32)
    scale = lax.rsqrt(jnp.mean(whole * whole, -1, keepdims=True) + 1e-06)
    nt[0, 0] = (whole * scale * gain_ref[...]).astype(BF)

    to_n = send(nt.at[0, 0], nt.at[0, 1], n_ss.at[0], n_rs.at[0], at_n)
    to_y = send(nt.at[0, 0], nt.at[0, 2], n_ss.at[1], n_rs.at[1], at_y)
    on_y = send(nt.at[0, 1], nt.at[0, 3], n_ss.at[2], n_rs.at[2], at_y)
    to_c = [send(nt.at[0, g], nt.at[1, g], n_ss.at[3 + g], n_rs.at[3 + g], at_c) for g in range(4)]
    to_n.start()
    to_y.start()
    to_c[0].start()
    pl.when(outer)(lambda: push(0, "f"))
    relay(1, "n")
    to_n.wait_recv()
    on_y.start()
    to_c[1].start()
    relay(0, "o")
    to_y.wait_recv()
    to_c[2].start()
    relay(0, "f", range(2))
    on_y.wait_recv()
    to_c[3].start()
    relay(0, "f", range(2, GCH))
    push(1, "o")
    push(1, "f")
    for copy in to_c:
        copy.wait_recv()
    for name in NAMES:
        crossed(0, name)

    depth = gu.shape[0] * gu.shape[1]

    def units(q, cols, size):
        both = jnp.dot(nt[q].reshape(4 * rows, model), gu[:, :, cols].reshape(depth, size), preferred_element_type=F32)
        gate = both[:, : size // 2]
        return (gate / (1.0 + jnp.exp(-gate)) * both[:, size // 2 :]).astype(BF)

    def hidden_of(q):
        def body(n, carry):
            cols = pl.ds(pl.multiple_of(n * 2 * LANES, 2 * LANES), 2 * LANES)
            hid[q, :, pl.ds(pl.multiple_of(n * LANES, LANES), LANES)] = units(q, cols, 2 * LANES)
            return carry

        lax.fori_loop(0, per, body, 0)
        hid[q, :, cut:] = units(q, pl.ds(edge, 2 * tail), 2 * tail)

    hidden_of(0)
    relay(1, "o")
    hidden_of(1)
    relay(1, "f")

    wide_d = dn.shape[2]
    order = [("s", 0), ("s", 1), ("n", 0), ("n", 1), ("o", 0), ("f", 0), ("o", 1), ("f", 1)]

    def slot_at(i):
        name, side = order[i]
        return 2 * dests[name] + (x if side == 0 else 1 - x)

    twin = [order.index(({"s": "n", "n": "s", "o": "f", "f": "o"}[name], side)) for name, side in order]

    def exchange(which, i):
        src, dst = ((c_send, c_recv), (s1, r1), (s2, r2))[which]
        on_z = which and (which == 1) == (order[i][1] == 1)
        there = twin[i] if on_z else i
        to = at_n if on_z else (at_y if which else at_c)
        return send(src.at[i], dst.at[there], e_ss.at[which, i], e_rs.at[which, there], to)

    def arrived(which, i):
        on_z = which and (which == 1) == (order[i][1] == 1)
        exchange(which, twin[i] if on_z else i).wait_recv()

    def lower(i):
        name, side = order[i]
        if side:
            crossed(1, name)
        slot = slot_at(i)
        c_send[i] = jnp.dot(hid[1], dn[slot], preferred_element_type=F32).astype(BF)
        exchange(0, i).start()
        acc[i] = jnp.dot(hid[0], dn[slot], preferred_element_type=F32).reshape(4, rows, wide_d)

    def first(i):
        arrived(0, i)
        both = acc[i] + c_recv[i].reshape(4, rows, wide_d).astype(F32)
        away = (1, 3) if order[i][1] else (2, 3)
        for j in range(2):
            s1[i, j] = both[away[j]].astype(BF)
        exchange(1, i).start()
        acc[i, 0] = both[0]
        acc[i, 1] = both[2 if order[i][1] else 1]

    def second(i):
        arrived(1, i)
        s2[i] = (acc[i, 1] + r1[i, 1].astype(F32)).astype(BF)
        exchange(2, i).start()

    def finish(i):
        arrived(2, i)
        cols = pl.ds(pl.multiple_of(slot_at(i) * wide_d, wide_d), wide_d)
        lowered = acc[i, 0] + r1[i, 0].astype(F32) + r2[i].astype(F32)
        out_ref[:, cols] = (mixed[:, cols].astype(F32) + 0.5 * lowered).astype(BF)

    count = len(order)
    for i in range(count + 1):
        if i < count:
            lower(i)
        if i > 0:
            first(i - 1)
        if i > 3:
            second(i - 4)
    for i in range(count - 3, count):
        second(i)
        if i < count - 1:
            finish(2 * (i - count + 3))
            finish(2 * (i - count + 3) + 1)
    for i in range(4, count):
        finish(i)

    for after, before in halos:
        pl.when(s < last)(after.wait_send)
        pl.when(s > 0)(before.wait_send)
    for kind in range(2):
        for name in NAMES:
            for g in range(chunks[kind]):
                by_x(kind, name, g).wait_send()
                if name != "s":
                    by_z(kind, name, g).wait_send()
    for m in range(2):
        for copy in (by_core(0, m), by_core(1, m), by_y(m)):
            copy.wait_send()
    for copy in [to_n, to_y, on_y] + to_c:
        copy.wait_send()
    for which in range(3):
        for i in range(len(order)):
            exchange(which, i).wait_send()


def local_lines(
    queries, keys, values, sink, stream, out_weight, norm_gain, gate_weight, up_weight, down_weight
):
    length = lax.axis_size("sp") // 2
    tokens = queries.shape[0]
    rows, model = stream.shape
    depth, wide = gate_weight.shape
    per = wide // LANES // 2
    tail = wide // 2 - per * LANES
    half = wide // 2
    slots = 2 * length
    part = down_weight.shape[1]
    blocks = tokens // WINDOW
    within, begins = turn_tables(slots * blocks + 2)
    vmem = pl.BlockSpec(memory_space=pltpu.VMEM)
    far = pl.BlockSpec(memory_space=pl.ANY)
    dma = pltpu.SemaphoreType.DMA
    dims = (length, tokens, rows, per, tail, tokens * slots)
    return pl.pallas_call(
        functools.partial(layer_kernel, dims),
        out_shape=jax.ShapeDtypeStruct((rows, model), BF),
        in_specs=[far] * 3 + [pl.BlockSpec(memory_space=pltpu.SMEM)] + [far] * 2 + [vmem] + [far] * 3 + [vmem] * 2,
        out_specs=vmem,
        scratch_shapes=[
            pltpu.VMEM(queries.shape, BF),
            pltpu.VMEM((tokens + 2 * WINDOW, 2 * LANES), BF),
            pltpu.VMEM((2, tokens + 2 * WINDOW, LANES), BF),
            pltpu.VMEM((2, tokens + 2 * WINDOW, LANES), BF),
            pltpu.VMEM(queries.shape, BF),
            pltpu.VMEM(out_weight.shape, BF),
            pltpu.VMEM(stream.shape, BF),
            pltpu.VMEM((2, depth, LANES), BF),
            pltpu.VMEM((depth, wide), BF),
            pltpu.VMEM((half, part), BF),
            pltpu.VMEM((slots, depth, wide), BF),
            pltpu.VMEM((slots, half, part), BF),
            pltpu.VMEM((2, rows, model), BF),
            pltpu.VMEM((2, rows, model), BF),
            pltpu.VMEM((2, 2, rows, model), F32),
            pltpu.VMEM((rows, model), BF),
            pltpu.VMEM((rows, model), BF),
            pltpu.VMEM((rows, model), BF),
            pltpu.VMEM((2, 4, rows, model), BF),
            pltpu.VMEM((2, 4 * rows, half), BF),
            pltpu.VMEM((slots, 4 * rows, part), BF),
            pltpu.VMEM((slots, 4 * rows, part), BF),
            pltpu.VMEM((slots, 4, rows, part), F32),
            pltpu.VMEM((slots, 2, rows, part), BF),
            pltpu.VMEM((slots, 2, rows, part), BF),
            pltpu.VMEM((slots, rows, part), BF),
            pltpu.VMEM((slots, rows, part), BF),
            dma((10,)), dma((2, 2)), dma((2, 2)),
            dma((2, 3, GCH)), dma((2, 4, GCH)), dma((slots, GCH)), dma((slots, DCH)),
            dma((3, 2)), dma((3, 2)), dma((7,)), dma((7,)), dma((3, slots)), dma((3, slots)),
        ],
        compiler_params=pltpu.CompilerParams(
            collective_id=0, has_side_effects=True, vmem_limit_bytes=63 * 1024 * 1024
        ),
    )(
        queries, keys, values, sink, stream, out_weight, norm_gain[None],
        gate_weight, up_weight, down_weight, jnp.asarray(within), jnp.asarray(begins),
    )


def solution(mesh):
    placed = (
        P("sp", "tp"),
        P("sp", "tp"),
        P("sp", "tp"),
        P("tp"),
        P(("sp", "tp"), None),
        P("tp", None),
        P(),
        P("sp", "tp"),
        P("sp", "tp"),
        P("tp", "sp"),
    )
    lines = mesh.shape["tp"] == 4 and mesh.shape["sp"] == 8
    return jax.shard_map(
        local_lines if lines else local, mesh=mesh, in_specs=placed, out_specs=P(("sp", "tp"), None), check_vma=False
    )
```

time: 178 us -> 145 us (0.81)
  Pallas kernels: 165 us -> 143 us
  other arithmetic: 6.66 us -> 0 us
  local copies, waits for them, and re-layouts: 5.93 us -> 1.98 us
    pallas_call x1, Pallas kernels: 165 us -> 143 us  [local_lines(): pl.pallas_call(functools.partial(layer_kernel, dims), out_shape=jax.Shape...]
    slice x5 -> x0, local copies, waits for them, and re-layouts: 3.35 us -> none  [the longest x1 1.18 us: lowers(): down_weight[at:at + per * LANES]]
    mul x1 -> x0, other arithmetic: 2.62 us -> none  [turn_tables(): return (jnp.cos(angles), jnp.sin(angles) * side[None, :])]
    select_n x3 -> x0, other arithmetic: 2.27 us -> none  [the longest x1 1.27 us: local_lines(): jnp.where(first, gu_1, gu_0)]
where the time goes in v1:
time: 145 us
  Pallas kernels  143 us (99%)
  local copies, waits for them, and re-layouts  1.98 us (1%)
    pallas_call x1, Pallas kernels, local_lines(): pl.pallas_call(functools.partial(layer_kernel, dims), out_shape=jax.Shape...  143 us

profile of v1, /device:TPU:0, one launch (start us, length us, event | category | flops | bytes accessed | tf_op | source)
XLA Modules:
  0.0 144.7 jit_solution(16162715201191399856)
XLA Ops:
  0.0 142.7 %shard_map.118 = bf16[160,2048]{1,0:T(8,128)(2,1)} custom-call(bf16[640,512]{1,0:T(8,128)(2,1)} %q_in.1, bf16[640,128]{1,0:T(8,128)(2,1)} %k_in.1, bf16[640,128]{1,0:T(8,128)(2,1)} %v_in.1, f32[8]{0:T(128)} %sink_ref.1, bf16[160,2048]{1,0:T(8,128)(2,1)} %stream_in.1, bf16[512,2048]{1,0:T(8,128)(2,1)} %w_in.1, f32[1,2048]{1,0:T(1,128)} %bitcast.1, ...), custom_call_target="tpu_custom_call" | custom-call | tf_op jit(solution)/shard_map/pallas_call | solution.py:579
  142.7 2.0 %copy.14 = bf16[160,2048]{1,0:T(8,128)(2,1)} copy(bf16[160,2048]{1,0:T(8,128)(2,1)} %shard_map.118) | data formatting | bytes 1310720

commit v2 on v1

--- a/solution.py
+++ b/solution.py
@@ -442,11 +442,11 @@
     to_y.wait_recv()
     to_c[2].start()
     relay(0, "f", range(2))
+    push(1, "o")
+    push(1, "f")
     on_y.wait_recv()
     to_c[3].start()
     relay(0, "f", range(2, GCH))
-    push(1, "o")
-    push(1, "f")
     for copy in to_c:
         copy.wait_recv()
     for name in NAMES:

time: 145 us -> 145 us (level)
  no operation moved by 1% of the time
where the time goes in v2:
time: 145 us
  Pallas kernels  143 us (99%)
  local copies, waits for them, and re-layouts  1.98 us (1%)
    pallas_call x1, Pallas kernels, local_lines(): pl.pallas_call(functools.partial(layer_kernel, dims), out_shape=jax.Shape...  143 us

profile of v2, /device:TPU:0, one launch (start us, length us, event | category | flops | bytes accessed | tf_op | source)
XLA Modules:
  0.0 144.7 jit_solution(5127778373010316708)
XLA Ops:
  0.0 142.7 %shard_map.118 = bf16[160,2048]{1,0:T(8,128)(2,1)} custom-call(bf16[640,512]{1,0:T(8,128)(2,1)} %q_in.1, bf16[640,128]{1,0:T(8,128)(2,1)} %k_in.1, bf16[640,128]{1,0:T(8,128)(2,1)} %v_in.1, f32[8]{0:T(128)} %sink_ref.1, bf16[160,2048]{1,0:T(8,128)(2,1)} %stream_in.1, bf16[512,2048]{1,0:T(8,128)(2,1)} %w_in.1, f32[1,2048]{1,0:T(1,128)} %bitcast.1, ...), custom_call_target="tpu_custom_call" | custom-call | tf_op jit(solution)/shard_map/pallas_call | solution.py:579
  142.7 2.0 %copy.14 = bf16[160,2048]{1,0:T(8,128)(2,1)} copy(bf16[160,2048]{1,0:T(8,128)(2,1)} %shard_map.118) | data formatting | bytes 1310720
